TPU v7x, 256 devices: a whole 4x4x8 slice. The times are simulated.
256 devices in a mesh: sp: 64 (over z, x, core), tp: 4 (over y).
Axes of the slice: x: 4, y: 4, z: 8, core: 2. Of those that a mesh axis runs over, the one named last changes fastest.
Arguments:
- x_res: bfloat16 [16384, 2048], P(('sp', 'tp')), may hold values from -6 to 6
- q_a: bfloat16 [16384, 1024], P('sp', 'tp'), may hold values from -48 to 48
- k_a: bfloat16 [16384, 256], P('sp', 'tp'), may hold values from -48 to 48
- v_a: bfloat16 [16384, 256], P('sp', 'tp'), may hold values from -6 to 6
- q_b: bfloat16 [16384, 1024], P('sp', 'tp'), may hold values from -48 to 48
- k_b: bfloat16 [16384, 512], P('sp', 'tp'), may hold values from -48 to 48
- v_b: bfloat16 [16384, 512], P('sp', 'tp'), may hold values from -6 to 6
- gain_qa: float32 [64], replicated, may hold values from 1.2 to 6
- gain_ka: float32 [64], replicated, may hold values from 1.2 to 6
- gain_qb: float32 [128], replicated, may hold values from 1.2 to 6
- gain_kb: float32 [128], replicated, may hold values from 1.2 to 6
- w_out_a: bfloat16 [1024, 2048], P('tp'), may hold values from -0.125 to 0.125
- w_out_b: bfloat16 [1024, 2048], P('tp'), may hold values from -0.125 to 0.125
- gain_mid: float32 [2048], replicated, may hold values from 0.1 to 1.9
- w_gate: bfloat16 [2048, 3072], P('sp', 'tp'), may hold values from -0.125 to 0.125
- w_up: bfloat16 [2048, 3072], P('sp', 'tp'), may hold values from -0.125 to 0.125
- conv_gate: float32 [3, 3072], P(None, 'tp'), may hold values from -3.5 to 3.5
- conv_up: float32 [3, 3072], P(None, 'tp'), may hold values from -3.5 to 3.5
- w_down: bfloat16 [3072, 2048], P('tp', 'sp'), may hold values from -0.109375 to 0.109375
Outputs:
- layer_out: bfloat16 [16384, 2048], P(('sp', 'tp'))
All inputs are finite; a program needn't handle non-finite values.
Results may differ from a plain program's by a relative error of at most 0.014.
The roundings to bfloat16 on the way count: a program that leaves them out, or rounds other values in their place, can miss the bound.
Values may be sent and summed in bfloat16 or wider, within the bound.
A program may use at most 128 MiB of HBM per device.

v0:
```python
import jax
import jax.numpy as jnp
from jax import lax
from jax.sharding import PartitionSpec as P

DHA = 64
DHB = 128


norm_eps = 1e-06
rope_theta = 10000.0


def gather_turned(arrays, axis, dims):
    turned = [jnp.moveaxis(a, dim, 0) for a, dim in zip(arrays, dims)]
    both = jnp.concatenate([t.reshape(len(t), -1) for t in turned], axis=1)
    result, at, gathered = (lax.all_gather(both, axis, axis=0, tiled=True), 0, [])
    for t, dim in zip(turned, dims):
        section = result[:, at : at + t[0].size].reshape(-1, *t.shape[1:])
        gathered.append(jnp.moveaxis(section, 0, dim))
        at += t[0].size
    return tuple(gathered)


def side_by_side(arrays, axis, dim, along):
    widths = [a.shape[along] for a in arrays]
    both = jnp.concatenate(arrays, axis=along)
    result = lax.all_gather(both, axis, axis=dim, tiled=True)
    return tuple(jnp.split(result, [sum(widths[:k]) for k in range(1, len(widths))], axis=along))


def cut_along(shard, dim, devices):
    dims = shard.shape
    parts = shard.reshape(*dims[:dim], devices, dims[dim] // devices, *dims[dim + 1 :])
    return jnp.moveaxis(parts, dim, 0)


def sent_and_summed(shard, axis, dim):
    parts = cut_along(shard, dim, lax.axis_size(axis))
    arrived = lax.all_to_all(parts, axis, split_axis=0, concat_axis=0, tiled=True)
    return arrived.astype(jnp.float32).sum(axis=0)


def joined_along(parts, dim):
    dims = list(parts.shape[1:])
    dims[dim] *= parts.shape[0]
    return jnp.moveaxis(parts, 0, dim).reshape(dims)


def sent_to_all(shard, axis):
    copies = jnp.broadcast_to(shard, (lax.axis_size(axis), *shard.shape))
    return lax.all_to_all(copies, axis, split_axis=0, concat_axis=0, tiled=True)


def gathered_copies(shard, axis, dim):
    return joined_along(sent_to_all(shard, axis), dim)


def extended(block, sides, width):
    for axis, dim in sides:
        count = lax.axis_size(axis)
        forward = [(i, i + 1) for i in range(count - 1)]
        backward = [(target, source) for source, target in forward]
        low = lax.ppermute(
            lax.slice_in_dim(block, block.shape[dim] - width, None, axis=dim), axis, forward
        )
        high = lax.ppermute(lax.slice_in_dim(block, 0, width, axis=dim), axis, backward)
        block = jnp.concatenate([low, block, high], axis=dim)
    return block


def rotary_angles(positions, head_size):
    half = head_size // 2
    inverse = jnp.power(jnp.float32(rope_theta), -jnp.arange(0, half, 2, dtype=jnp.float32) / half)
    grid_row = (positions // 64).astype(jnp.float32)[:, None] * inverse[None, :]
    grid_col = (positions % 64).astype(jnp.float32)[:, None] * inverse[None, :]
    angles = jnp.concatenate([grid_row, grid_row, grid_col, grid_col], axis=-1)
    return (jnp.cos(angles), jnp.sin(angles))


def rotate_half(values):
    first, second = jnp.split(values, 2, axis=-1)
    return jnp.concatenate([-second, first], axis=-1)


def prepare(raw, gain, head_size, positions):
    count = raw.shape[0]
    heads = raw.shape[1] // head_size
    values = raw.astype(jnp.float32).reshape(count, heads, head_size)
    values = values * lax.rsqrt(jnp.mean(values * values, axis=-1, keepdims=True) + norm_eps)
    values = values * gain
    cosine, sine = rotary_angles(positions, head_size)
    row_part, col_part = jnp.split(values, 2, axis=-1)
    turned = jnp.concatenate([rotate_half(row_part), rotate_half(col_part)], axis=-1)
    values = values * cosine[:, None, :] + turned * sine[:, None, :]
    return values.astype(jnp.bfloat16)


def start_state(queries):
    count, kv_heads, groups, head_size = queries.shape
    lowest = jnp.full((kv_heads, groups, count), -1e30, jnp.float32)
    totals = jnp.zeros((kv_heads, groups, count), jnp.float32)
    summed = jnp.zeros((kv_heads, groups, count, head_size), jnp.float32)
    return (lowest, totals, summed)


def attend(state, queries, key_piece, value_piece):
    head_size = queries.shape[3]
    kv_heads = queries.shape[1]
    length = key_piece.shape[0]
    keys = key_piece.reshape(length, kv_heads, head_size)
    values = value_piece.reshape(length, kv_heads, head_size)
    span = length
    while span > 1024 and span % 2 == 0:
        span = span // 2
    scale = jnp.float32(head_size ** (-0.5))

    def one_span(index, carry):
        running, totals, summed = carry
        key_rows = lax.dynamic_slice_in_dim(keys, index * span, span, 0)
        value_rows = lax.dynamic_slice_in_dim(values, index * span, span, 0)
        scores = (
            jnp.einsum("qkgd,skd->kgqs", queries, key_rows, preferred_element_type=jnp.float32)
            * scale
        )
        highest = jnp.maximum(running, jnp.max(scores, axis=-1))
        factor = jnp.exp(running - highest)
        expd = jnp.exp(scores - highest[..., None])
        totals = totals * factor + jnp.sum(expd, axis=-1)
        summed = summed * factor[..., None] + jnp.einsum(
            "kgqs,skd->kgqd",
            expd.astype(jnp.bfloat16),
            value_rows,
            preferred_element_type=jnp.float32,
        )
        return (highest, totals, summed)

    return lax.fori_loop(0, length // span, one_span, state)


def finish(state):
    running, totals, summed = state
    kv_heads, groups, count, head_size = summed.shape
    result = summed / totals[..., None]
    return (
        jnp.transpose(result, (2, 0, 1, 3))
        .reshape(count, kv_heads * groups * head_size)
        .astype(jnp.bfloat16)
    )


def on_device(
    x_res,
    q_a,
    k_a,
    v_a,
    q_b,
    k_b,
    v_b,
    gain_qa,
    gain_ka,
    gain_qb,
    gain_kb,
    w_out_a,
    w_out_b,
    gain_mid,
    w_gate,
    w_up,
    conv_gate,
    conv_up,
    w_down,
):
    tok_rows = q_a.shape[0]
    whole_gate, whole_up, whole_down = gather_turned((w_gate, w_up, w_down), "sp", (0, 0, 1))
    positions = lax.axis_index("sp") * tok_rows + lax.iota(jnp.int32, tok_rows)
    kv_a = k_a.shape[1] // DHA
    kv_b = k_b.shape[1] // DHB
    query_a = prepare(q_a, gain_qa, DHA, positions)
    query_a = query_a.reshape(tok_rows, kv_a, query_a.shape[1] // kv_a, DHA)
    query_b = prepare(q_b, gain_qb, DHB, positions)
    query_b = query_b.reshape(tok_rows, kv_b, query_b.shape[1] // kv_b, DHB)
    keys_a = prepare(k_a, gain_ka, DHA, positions).reshape(tok_rows, kv_a * DHA)
    keys_b = prepare(k_b, gain_kb, DHB, positions).reshape(tok_rows, kv_b * DHB)
    pieces = side_by_side((keys_a, v_a), "sp", 0, 1)
    state_a = attend(start_state(query_a), query_a, pieces[0], pieces[1])
    pieces = side_by_side((keys_b, v_b), "sp", 0, 1)
    state_b = attend(start_state(query_b), query_b, pieces[0], pieces[1])
    attn_a = finish(state_a)
    attn_b = finish(state_b)
    projected = sent_and_summed(
        (
            jnp.dot(attn_a, w_out_a, preferred_element_type=jnp.float32)
            + jnp.dot(attn_b, w_out_b, preferred_element_type=jnp.float32)
        ).astype(jnp.bfloat16),
        "tp",
        0,
    )
    middle = x_res.astype(jnp.float32) + projected
    normed = middle * lax.rsqrt(jnp.mean(middle * middle, axis=-1, keepdims=True) + norm_eps)
    normed = (normed * gain_mid).astype(jnp.bfloat16)
    gathered = gathered_copies(normed, "tp", 0)
    gate_pre = jnp.dot(gathered, whole_gate, preferred_element_type=jnp.float32)
    up_pre = jnp.dot(gathered, whole_up, preferred_element_type=jnp.float32)
    width = gate_pre.shape[1]
    joined = jnp.concatenate([gate_pre, up_pre], axis=1).astype(jnp.bfloat16)
    padded = extended(joined, (("sp", 0),), 1)
    taps = jnp.concatenate([conv_gate, conv_up], axis=1)
    mixed = padded[:-2] * taps[0] + padded[1:-1] * taps[1] + padded[2:] * taps[2]
    hidden = (jax.nn.silu(mixed[:, :width]) * mixed[:, width:]).astype(jnp.bfloat16)
    terms = jnp.dot(hidden, whole_down, preferred_element_type=jnp.float32)
    summed = sent_and_summed(terms.astype(jnp.bfloat16), "tp", 0)
    return (middle + summed).astype(jnp.bfloat16)


def solution(mesh):
    in_specs = (
        P(("sp", "tp"), None),
        P("sp", "tp"),
        P("sp", "tp"),
        P("sp", "tp"),
        P("sp", "tp"),
        P("sp", "tp"),
        P("sp", "tp"),
        P(),
        P(),
        P(),
        P(),
        P("tp", None),
        P("tp", None),
        P(),
        P("sp", "tp"),
        P("sp", "tp"),
        P(None, "tp"),
        P(None, "tp"),
        P("tp", "sp"),
    )
    out_specs = P(("sp", "tp"), None)
    return jax.shard_map(
        on_device, mesh=mesh, in_specs=in_specs, out_specs=out_specs, check_vma=False
    )
```

profile of v0, /device:TPU:1, one launch (start us, length us, event | category | flops | bytes accessed | tf_op | source)
XLA Modules:
  0.0 368.4 jit_solution(727148971909059636)
XLA Ops:
  16.5 74.8 %all-gather.4.cloned.1.call-done = bf16[16384,128]{0,1:T(8,128)(2,1)} async-done(((bf16[256,128]{0,1:T(8,128)(2,1)}), bf16[16384,128]{0,1:T(8,128)(2,1)}) %all-gather.4.cloned.1.call-update) | async-done | bytes 4194320 | tf_op jit(solution)/shard_map/all_gather | solution.py:28
  91.3 4.6 %slice_bitcast_fusion.2 = (bf16[16384,1,64]{0,2,1:T(8,128)(2,1)}, bf16[16384,1,64]{0,2,1:T(8,128)(2,1)}) fusion(bf16[16384,128]{0,1:T(8,128)(2,1)} %all-gather.4.cloned.1.call-done), kind=kLoop, calls=%fused_computation.61 | loop fusion | bytes 8388608 | tf_op jit(solution)/shard_map/reshape | solution.py:112
  95.9 127.8 %while.36 = (s32[]{:T(128)}, f32[1,4,256]{2,1,0:T(4,128)S(1)}, f32[1,4,256]{2,1,0:T(4,128)S(1)}, f32[1,4,256,64]{2,3,1,0:T(8,128)S(1)}, bf16[16384,1,64]{0,2,1:T...) while((s32[]{:T(128)}, f32[1,4,256]{2,1,0:T(4,128)S(1)}, ...), condition=%wide.region_5.6_spmd.clone, body=%wide.region_2.5_spmd.clone.sunk | while | flops 277026816 | bytes 30343368 | solution.py:138
  103.8 3.6 bitcast_reduce_fusion.4
  111.7 3.6 bitcast_reduce_fusion.4
  119.7 3.6 bitcast_reduce_fusion.4
  127.6 3.6 bitcast_reduce_fusion.4
  135.6 3.6 bitcast_reduce_fusion.4
  143.5 3.6 bitcast_reduce_fusion.4
  151.7 3.6 bitcast_reduce_fusion.4
  160.0 3.6 bitcast_reduce_fusion.4
  168.1 3.7 bitcast_reduce_fusion.4
  176.0 3.6 bitcast_reduce_fusion.4
  184.0 3.6 bitcast_reduce_fusion.4
  192.0 3.6 bitcast_reduce_fusion.4
  199.9 3.6 bitcast_reduce_fusion.4
  207.9 3.6 bitcast_reduce_fusion.4
  215.8 3.6 bitcast_reduce_fusion.4
  225.5 5.9 %slice_bitcast_fusion = (bf16[16384,1,128]{2,0,1:T(8,128)(2,1)}, bf16[16384,1,128]{2,0,1:T(8,128)(2,1)}) fusion(bf16[16384,256]{1,0:T(8,128)(2,1)} %all-gather.6.cloned.1.call-done), kind=kLoop, calls=%fused_computation.50 | loop fusion | bytes 16777216 | tf_op jit(solution)/shard_map/reshape | solution.py:112
  231.4 53.4 %while.37 = (s32[]{:T(128)}, f32[1,2,256]{2,1,0:T(2,128)S(1)}, f32[1,2,256]{2,1,0:T(2,128)S(1)}, f32[1,2,256,128]{3,2,1,0:T(8,128)S(1)}, bf16[16384,1,128]{2,0,1...) while((s32[]{:T(128)}, f32[1,2,256]{2,1,0:T(2,128)S(1)}, ...), condition=%wide.region_11.12_spmd.clone, body=%wide.region_8.11_spmd.clone.sunk | while | flops 272829440 | bytes 7504047 | solution.py:138
  287.4 18.9 %all_to_all.15 = bf16[4,64,2048]{2,1,0:T(8,128)(2,1)S(1)} all-to-all(bf16[4,64,2048]{2,1,0:T(8,128)(2,1)S(1)} %bitcast.212), channel_id=1, replica_groups=mesh['sp'=64,'tp'=4] {'tp'}, dimensions={0} | all-to-all | bytes 2097152 | tf_op jit(solution)/shard_map/all_to_all | solution.py:40
  311.5 14.0 %all-to-all-done.1 = bf16[4,64,2048]{2,1,0:T(8,128)(2,1)S(1)} async-done(((bf16[4,64,2048]{2,1,0:T(8,128)(2,1)}), bf16[4,64,2048]{2,1,0:T(8,128)(2,1)S(1)}, u32[]{:S(2)}, u32[]{:S(2)}) %all-to-all-start.1) | async-done | bytes 1048608 | tf_op jit(solution)/shard_map/all_to_all | solution.py:52
  331.2 5.0 %collective-permute-start = (bf16[1,1536]{1,0:T(2,128)(2,1)S(1)}, bf16[1,1536]{1,0:T(2,128)(2,1)S(1)}, u32[]{:S(2)}, u32[]{:S(2)}) collective-permute-start(bf16[1,1536]{1,0:T(2,128)(2,1)S(1)} %get-tuple-element.360), channel_id=1, source_target_pairs={{0,4},{4,8},{8,12},{12,16},{16,20},{20,24},{24,28},{28,32},{32,36}... | collective-permute-start | bytes 9224 | tf_op jit(solution)/shard_map/ppermute | solution.py:64
  344.6 16.4 %all_to_all.16 = bf16[4,64,2048]{2,1,0:T(8,128)(2,1)S(1)} all-to-all(bf16[4,64,2048]{2,1,0:T(8,128)(2,1)S(1)} %bitcast.220), channel_id=1, replica_groups=mesh['sp'=64,'tp'=4] {'tp'}, dimensions={0} | all-to-all | bytes 2097152 | tf_op jit(solution)/shard_map/all_to_all | solution.py:40
  (310 shorter events, 159.2 us)
Async XLA Ops:
  6.5 217.2 %copy-start = (bf16[256,2048]{1,0:T(8,128)(2,1)S(1)}, bf16[256,2048]{1,0:T(8,128)(2,1)}, u32[]{:S(2)}) copy-start(bf16[256,2048]{1,0:T(8,128)(2,1)} %param.34) | copy-start | bytes 3145732
  6.5 6.6 %copy-start.3 = (bf16[256,128]{1,0:T(8,128)(2,1)S(1)}, bf16[256,128]{1,0:T(8,128)(2,1)}, u32[]{:S(2)}) copy-start(bf16[256,128]{1,0:T(8,128)(2,1)} %param.28) | copy-start | bytes 196612
  6.5 6.6 %copy-start.13 = (f32[128]{0:T(128)S(1)}, f32[128]{0:T(128)}, u32[]{:S(2)}) copy-start(f32[128]{0:T(128)} %param.33) | copy-start | bytes 1540
  6.5 7.3 %copy-start.6 = (bf16[256,128]{1,0:T(8,128)(2,1)S(1)}, bf16[256,128]{1,0:T(8,128)(2,1)}, u32[]{:S(2)}) copy-start(bf16[256,128]{1,0:T(8,128)(2,1)} %param.29) | copy-start | bytes 196612
  6.5 8.0 %copy-start.7 = (bf16[768,32]{0,1:T(8,128)(2,1)S(1)}, bf16[768,32]{0,1:T(8,128)(2,1)}, u32[]{:S(2)}) copy-start(bf16[768,32]{0,1:T(8,128)(2,1)} %param.41) | copy-start | bytes 147460
  6.5 8.0 %copy-start.9 = (bf16[32,768]{1,0:T(8,128)(2,1)S(1)}, bf16[32,768]{1,0:T(8,128)(2,1)}, u32[]{:S(2)}) copy-start(bf16[32,768]{1,0:T(8,128)(2,1)} %param.37) | copy-start | bytes 147460
  6.6 8.0 %copy-start.8 = (bf16[32,768]{1,0:T(8,128)(2,1)S(1)}, bf16[32,768]{1,0:T(8,128)(2,1)}, u32[]{:S(2)}) copy-start(bf16[32,768]{1,0:T(8,128)(2,1)} %param.38) | copy-start | bytes 147460
  6.6 84.7 %all-gather.4.cloned.1.call-start = ((), (), s32[]{:S(2)}) async-start(), calls=%async_computation.3 | async-start | bytes 4259840 | tf_op jit(solution)/shard_map/all_gather | solution.py:28
  10.8 4.7 %copy-start.5 = (bf16[256,256]{1,0:T(8,128)(2,1)S(1)}, bf16[256,256]{1,0:T(8,128)(2,1)}, u32[]{:S(2)}) copy-start(bf16[256,256]{1,0:T(8,128)(2,1)} %param.27) | copy-start | bytes 393220
  10.8 214.7 %all-gather.6.cloned.1.call-start = ((), (), s32[]{:S(2)}) async-start(), calls=%async_computation.4 | async-start | bytes 8519680 | tf_op jit(solution)/shard_map/all_gather | solution.py:28
  14.5 310.9 %all-gather.8.cloned.1.call-start = ((), (), s32[]{:S(2)}) async-start(), calls=%async_computation.5 | async-start | bytes 9584640 | tf_op jit(solution)/shard_map/all_gather | solution.py:17
  115.4 3.6 copy-start.1
  147.2 3.8 %copy-start.1 = (f32[1024,256,4]{1,0,2:T(8,128)S(1)}, f32[1024,256,4]{1,0,2:T(8,128)}, u32[]{:S(2)}) copy-start(f32[1024,256,4]{1,0,2:T(8,128)} %get-tuple-element.476) | copy-start | bytes 12582916 | tf_op jit(solution)/shard_map/while
  155.4 3.9 %copy-start.1 = (f32[1024,256,4]{1,0,2:T(8,128)S(1)}, f32[1024,256,4]{1,0,2:T(8,128)}, u32[]{:S(2)}) copy-start(f32[1024,256,4]{1,0,2:T(8,128)} %get-tuple-element.476) | copy-start | bytes 12582916 | tf_op jit(solution)/shard_map/while
  163.7 3.6 copy-start.1
  187.6 3.6 copy-start.1
  195.6 3.5 copy-start.1
  287.4 19.1 %copy-start.2 = (bf16[64,2048]{1,0:T(8,128)(2,1)S(1)}, bf16[64,2048]{1,0:T(8,128)(2,1)}, u32[]{:S(2)}) copy-start(bf16[64,2048]{1,0:T(8,128)(2,1)} %param.23) | copy-start | bytes 786436
  287.4 19.3 %copy-start.12 = (f32[2048]{0:T(1024)S(1)}, f32[2048]{0:T(1024)}, u32[]{:S(2)}) copy-start(f32[2048]{0:T(1024)} %param.36) | copy-start | bytes 24580
  306.7 4.8 %copy-start.10 = (f32[3,768]{1,0:T(4,128)S(1)}, f32[3,768]{1,0:T(4,128)}, u32[]{:S(2)}) copy-start(f32[3,768]{1,0:T(4,128)} %param.39) | copy-start | bytes 27652
  306.7 4.8 %copy-start.11 = (f32[3,768]{1,0:T(4,128)S(1)}, f32[3,768]{1,0:T(4,128)}, u32[]{:S(2)}) copy-start(f32[3,768]{1,0:T(4,128)} %param.40) | copy-start | bytes 27652
  307.9 17.6 %all-to-all-start.1 = ((bf16[4,64,2048]{2,1,0:T(8,128)(2,1)}), bf16[4,64,2048]{2,1,0:T(8,128)(2,1)S(1)}, u32[]{:S(2)}, u32[]{:S(2)}) async-start(bf16[4,64,2048]{2,1,0:T(8,128)(2,1)} %broadcast_in_dim.28), calls=%async_computation.1 | async-start | bytes 2097152 | tf_op jit(solution)/shard_map/all_to_all | solution.py:52
  331.2 7.0 %collective-permute-start = (bf16[1,1536]{1,0:T(2,128)(2,1)S(1)}, bf16[1,1536]{1,0:T(2,128)(2,1)S(1)}, u32[]{:S(2)}, u32[]{:S(2)}) collective-permute-start(bf16[1,1536]{1,0:T(2,128)(2,1)S(1)} %get-tuple-element.360), channel_id=1, source_target_pairs={{0,4},{4,8},{8,12},{12,16},{16,20},{20,24},{24,28},{28,32},{32,36}... | collective-permute-start | bytes 9224 | tf_op jit(solution)/shard_map/ppermute | solution.py:64
  336.2 4.9 %collective-permute-start.1 = (bf16[1,1536]{1,0:T(2,128)(2,1)S(1)}, bf16[1,1536]{1,0:T(2,128)(2,1)S(1)}, u32[]{:S(2)}, u32[]{:S(2)}) collective-permute-start(bf16[1,1536]{1,0:T(2,128)(2,1)S(1)} %get-tuple-element.361), channel_id=1, source_target_pairs={{4,0},{8,4},{12,8},{16,12},{20,16},{24,20},{28,24},{32,28},{36,32}... | collective-permute-start | bytes 9224 | tf_op jit(solution)/shard_map/ppermute | solution.py:67
  (13 other events, 42.2 us)
Sparse Core Ops, SparseCore 0:
  10.9 80.2 all-gather.3
  94.0 82.3 all-gather.5
  179.2 80.8 all-gather.7
where the time goes:
time: 371 us; the launch traced here: 368 us
  matrix products  170 us (46%)
  waiting for transfers between devices  91.8 us (25%)
  blocking collectives  35.3 us (10%)
  other arithmetic  28.9 us (8%)
  local copies, waits for them, and re-layouts  16.6 us (4%)
  between operations  13.7 us (4%)
  starting transfers between devices  10.5 us (3%)
    dot_general x32, matrix products, one_span(): jnp.einsum('qkgd,skd->kgqs', queries, key_rows, preferred_element_type=jn...  80.8 us
    dot_general x32, matrix products, one_span(): jnp.einsum('kgqs,skd->kgqd', expd.astype(jnp.bfloat16), value_rows, prefe...  76.7 us
    all_gather x2, waiting for transfers between devices, side_by_side(): result = lax.all_gather(both, axis, axis=dim, tiled=True)  74.8 us
    all_to_all x2, blocking collectives, sent_and_summed(): lax.all_to_all(parts, axis, split_axis=0, concat_axis=0, tiled=True)  35.3 us
    reduce_sum x32, other arithmetic, one_span(): totals = totals * factor + jnp.sum(expd, axis=-1)  17.1 us
    all_to_all x1, waiting for transfers between devices, sent_to_all(): return lax.all_to_all(copies, axis, split_axis=0, concat_axis=0, tiled=True)  14 us
    reshape x2, local copies, waits for them, and re-layouts, attend(): values = value_piece.reshape(length, kv_heads, head_size)  10.5 us
  transfers between devices with their start and end apart: 6, of which 3 were waited for; matrix products, arithmetic and copies ran while one was open for 54% of the time, Pallas kernels for 0%

commit v1 on v0

v1 whole, which is shorter than its diff:
```python
import functools
import math

import jax
import jax.numpy as jnp
from jax import lax
from jax.experimental import pallas as pl
from jax.experimental.pallas import tpu as pltpu
from jax.sharding import PartitionSpec as P

DHA = 64
DHB = 128
NZ = 8
NX = 4
NY = 4
NSETS = NZ
MESH = pl.DeviceIdType.MESH
F32 = jnp.float32
BF16 = jnp.bfloat16
LOG2E = math.log2(math.e)

norm_eps = 1e-06
rope_theta = 10000.0


def rotary_angles(positions, head_size):
    half = head_size // 2
    inverse = jnp.power(jnp.float32(rope_theta), -jnp.arange(0, half, 2, dtype=jnp.float32) / half)
    grid_row = (positions // 64).astype(jnp.float32)[:, None] * inverse[None, :]
    grid_col = (positions % 64).astype(jnp.float32)[:, None] * inverse[None, :]
    angles = jnp.concatenate([grid_row, grid_row, grid_col, grid_col], axis=-1)
    return (jnp.cos(angles), jnp.sin(angles))


def rotate_half(values):
    first, second = jnp.split(values, 2, axis=-1)
    return jnp.concatenate([-second, first], axis=-1)


def prepare(raw, gain, head_size, positions):
    count = raw.shape[0]
    heads = raw.shape[1] // head_size
    values = raw.astype(jnp.float32).reshape(count, heads, head_size)
    values = values * lax.rsqrt(jnp.mean(values * values, axis=-1, keepdims=True) + norm_eps)
    values = values * gain
    cosine, sine = rotary_angles(positions, head_size)
    row_part, col_part = jnp.split(values, 2, axis=-1)
    turned = jnp.concatenate([rotate_half(row_part), rotate_half(col_part)], axis=-1)
    values = values * cosine[:, None, :] + turned * sine[:, None, :]
    return values.astype(jnp.bfloat16)


class Place:
    def __init__(self):
        self.sp = lax.axis_index("sp")
        self.y = lax.axis_index("tp")
        self.c = self.sp % 2
        self.x = (self.sp // 2) % NX
        self.z = self.sp // (2 * NX)
        self.s = 1 - 2 * self.c

    def at(self, z, x, c):
        return (z * NX + x) * 2 + c

    def zz(self, d):
        return (self.z + d + 2 * NZ) % NZ

    def xx(self, d):
        return (self.x + d + 2 * NX) % NX

    def set_z(self, t, s):
        k = (t + 1) // 2
        sign = 1 - 2 * (t % 2)
        return self.zz(sign * s * k)


class Gather:
    def __init__(self, place, group_a, piece_a, piece_b, sems):
        self.p = place
        self.group_a, self.piece_a, self.piece_b = group_a, piece_a, piece_b
        (self.ax_s, self.ax_r, self.az_s, self.az_r, self.at_s, self.at_r,
         self.bz_s, self.bz_r, self.bx_s, self.bx_r, self.bt_s, self.bt_r) = sems

    def _copy(self, ref, s_sem, r_sem, sp):
        return pltpu.make_async_remote_copy(
            src_ref=ref, dst_ref=ref, send_sem=s_sem, recv_sem=r_sem,
            device_id={"sp": sp}, device_id_type=MESH,
        )

    def c_ax(self, k):
        p = self.p
        src_x = [p.x, p.xx(-p.s), p.x][k]
        to = [p.xx(p.s), p.xx(p.s), p.xx(-p.s)][k]
        return self._copy(self.piece_a(p.z, src_x, p.c), self.ax_s.at[k], self.ax_r.at[k], p.at(p.z, to, p.c))

    def c_az(self, t, to_z, src_z):
        p = self.p
        return self._copy(self.group_a(src_z, p.c), self.az_s.at[t], self.az_r.at[t], p.at(to_z, p.x, p.c))

    def c_at(self, t):
        p = self.p
        return self._copy(self.group_a(p.set_z(t, p.s), p.c), self.at_s.at[t], self.at_r.at[t], p.at(p.z, p.x, 1 - p.c))

    def c_bz(self, t, to_z, src_z):
        p = self.p
        return self._copy(self.piece_b(src_z, p.x, p.c), self.bz_s.at[t], self.bz_r.at[t], p.at(to_z, p.x, p.c))

    def c_bx(self, t, k):
        p = self.p
        src_x = [p.x, p.xx(-p.s), p.x][k]
        to = [p.xx(p.s), p.xx(p.s), p.xx(-p.s)][k]
        return self._copy(self.piece_b(p.set_z(t, p.s), src_x, p.c), self.bx_s.at[t, k], self.bx_r.at[t, k],
                          p.at(p.z, to, p.c))

    def c_bt(self, t, k):
        p = self.p
        src_x = [p.x, p.xx(-p.s), p.xx(p.s), p.xx(-2 * p.s)][k]
        return self._copy(self.piece_b(p.set_z(t, p.s), src_x, p.c), self.bt_s.at[t, k], self.bt_r.at[t, k],
                          p.at(p.z, p.x, 1 - p.c))

    def start_b(self):
        p = self.p
        self.c_bz(1, p.zz(p.s), p.z).start()
        self.c_bz(2, p.zz(-p.s), p.z).start()
        self.c_bx(0, 0).start()
        self.c_bx(0, 2).start()
        self.c_bt(0, 0).start()

    def start_a(self):
        self.c_ax(0).start()
        self.c_ax(2).start()

    def x_a(self):
        p = self.p
        self.c_ax(0).wait_recv()
        self.c_ax(1).start()
        self.c_ax(2).wait_recv()
        self.c_ax(1).wait_recv()
        self.c_az(1, p.zz(p.s), p.z).start()
        self.c_az(2, p.zz(-p.s), p.z).start()
        self.c_at(0).start()

    def _hop(self, t, copy):
        p = self.p
        sign = (2 * (t % 2) - 1) * p.s
        copy(t, p.z, p.set_z(t, p.s)).wait_recv()

        @pl.when(t <= NSETS - 3)
        def _():
            copy(t + 2, p.zz(sign), p.set_z(t, p.s)).start()

    def z_b(self, t):
        self._hop(t, self.c_bz)
        self.c_bx(t, 0).start()
        self.c_bx(t, 2).start()
        self.c_bt(t, 0).start()

    def z_a(self, t):
        self._hop(t, self.c_az)
        self.c_at(t).start()

    def x1(self, t):
        self.c_bx(t, 0).wait_recv()
        self.c_bx(t, 1).start()
        self.c_bt(t, 1).start()

    def x2(self, t):
        self.c_bx(t, 2).wait_recv()
        self.c_bt(t, 2).start()

    def x3(self, t):
        self.c_bx(t, 1).wait_recv()
        self.c_bt(t, 3).start()

    def arrived(self, t):
        self.c_at(t).wait_recv()
        for k in range(4):
            self.c_bt(t, k).wait_recv()

    def drain(self):
        p = self.p
        for k in range(3):
            self.c_ax(k).wait_send()

        @pl.loop(0, NSETS)
        def _(t):
            self.c_at(t).wait_send()
            for k in range(3):
                self.c_bx(t, k).wait_send()
            for k in range(4):
                self.c_bt(t, k).wait_send()

            @pl.when(t >= 1)
            def _():
                self.c_az(t, p.z, p.z).wait_send()
                self.c_bz(t, p.z, p.z).wait_send()


def gather_sems():
    d = pltpu.SemaphoreType.DMA
    return [d((3,)), d((3,)), d((8,)), d((8,)), d((8,)), d((8,)),
            d((8,)), d((8,)), d((8, 3)), d((8, 3)), d((8, 4)), d((8, 4))]


def dot(a, b):
    return jnp.dot(a, b, preferred_element_type=F32)


def kernel(kva_h, kvb_h, qa_ref, qb_ref, wgu_h, wd_h, woa_h, wob_h, x_ref, gain_ref, cg_ref, cu_ref, out_ref,
           ba, bb, wgu, wd, woa, wob, s_a, s_b, p_ref, acc_a, acc_b, mx,
           attn, part, rs_mid, rs_in, mid, ag, pre, halo, hid, part2, rs_mid2, rs_in2,
           loc, wo_sem, rs_s, rs_r, rs_s2, rs_r2, ag_s, ag_r, h_s, h_r, *sems):
    p = Place()
    n = len(sems) // 2

    barrier = pltpu.get_barrier_semaphore()
    up, down = (p.y + 1) % NY, (p.y + NY - 1) % NY
    opp = (p.y + 2) % NY
    sp_next, sp_prev = (p.sp + 1) % 64, (p.sp + 63) % 64
    own_a = pltpu.make_async_copy(kva_h, ba.at[p.c, p.z, p.x], loc.at[0])
    own_b = pltpu.make_async_copy(kvb_h, bb.at[p.c, p.z, p.x], loc.at[1])
    own_gu = pltpu.make_async_copy(wgu_h, wgu.at[p.z * NX + p.x, p.c], loc.at[2])
    own_d = pltpu.make_async_copy(wd_h, wd.at[p.z * NX + p.x, p.c], loc.at[3])
    own_oa = pltpu.make_async_copy(woa_h, woa, wo_sem.at[0])
    own_ob = pltpu.make_async_copy(wob_h, wob, wo_sem.at[1])
    for copy in (own_b, own_a, own_gu, own_d, own_oa, own_ob):
        copy.start()
    greeted = [p.at(p.zz(1), p.x, p.c), p.at(p.zz(-1), p.x, p.c), p.at(p.z, p.xx(1), p.c), p.at(p.z, p.xx(-1), p.c),
               p.at(p.z, p.x, 1 - p.c), sp_next, sp_prev]
    for sp in greeted:
        pl.semaphore_signal(barrier, inc=1, device_id={"sp": sp}, device_id_type=MESH)
    for y in (up, down):
        pl.semaphore_signal(barrier, inc=1, device_id={"tp": y}, device_id_type=MESH)
    pl.semaphore_wait(barrier, 9)

    g = Gather(p, lambda z, c: ba.at[c, z], lambda z, x, c: ba.at[c, z, x], lambda z, x, c: bb.at[c, z, x], sems[:n])
    w = Gather(p, lambda z, c: wgu.at[pl.ds(z * NX, NX), c], lambda z, x, c: wgu.at[z * NX + x, c],
               lambda z, x, c: wd.at[z * NX + x, c], sems[n:])

    own_b.wait()
    g.start_b()
    own_a.wait()
    g.start_a()
    own_gu.wait()
    own_d.wait()
    acc_a[...] = jnp.zeros_like(acc_a)
    acc_b[...] = jnp.zeros_like(acc_b)
    mx[...] = jnp.full_like(mx, -1e30)
    g.x_a()
    g.x1(0)
    g.x2(0)
    g.x3(0)
    g.arrived(0)

    zeros64 = jnp.zeros((64, 256), BF16)

    def scores(tile, buf, parts):
        top = None
        if tile < 4:
            q = qa_ref[tile]
            both = (jnp.concatenate([q, zeros64], axis=0), jnp.concatenate([zeros64, q], axis=0))
            for i, (cc, z) in enumerate(parts):
                keys = ba[cc, z, :, 0:128, :].reshape(512, 128)
                for h in range(2):
                    sc = dot(keys, both[h])
                    buf[pl.ds((i * 2 + h) * 512, 512), :] = sc
                    m8 = jnp.max(sc.reshape(64, 8, 256), axis=0)
                    top = m8 if top is None else jnp.maximum(top, m8)
        else:
            q = qb_ref[tile - 4]
            for i, (cc, z) in enumerate(parts):
                for h in range(2):
                    keys = bb[cc, z, 2 * h:2 * h + 2, 0:256, :].reshape(512, 128)
                    sc = dot(keys, q)
                    buf[pl.ds((i * 2 + h) * 512, 512), :] = sc
                    m8 = jnp.max(sc.reshape(64, 8, 256), axis=0)
                    top = m8 if top is None else jnp.maximum(top, m8)
        return jnp.max(top, axis=0, keepdims=True)

    def weigh(tile, buf, top, parts):
        scale = LOG2E if tile < 4 else LOG2E * DHB ** -0.5
        old = mx[tile]
        new = jnp.maximum(old, top * scale)
        mx[tile] = new
        factor = jnp.exp2(old - new)
        total = None
        for i, (cc, z) in enumerate(parts):
            for h in range(2):
                rows = pl.ds((i * 2 + h) * 512, 512)
                p_ref[rows, :] = jnp.exp2(buf[rows, :] * scale - new).astype(BF16)
                if tile < 4:
                    vt = jnp.concatenate([ba[cc, z, x, 128 + 64 * h:192 + 64 * h, :] for x in range(4)], axis=1)
                else:
                    vt = jnp.concatenate(
                        [bb[cc, z, x, 256 + 128 * e:384 + 128 * e, :] for x in (2 * h, 2 * h + 1) for e in range(2)], axis=1)
                vt = jnp.concatenate([vt, jnp.ones((16, 512), BF16)], axis=0)
                o = dot(vt, p_ref[rows, :])
                total = o if total is None else total + o
        if tile < 4:
            acc_a[tile] = acc_a[tile] * factor + total
        else:
            acc_b[tile - 4] = acc_b[tile - 4] * factor + total

    @pl.loop(1, NSETS + 1)
    def _(t):
        last = t == NSETS
        odd = t % 2 == 1
        parts = ((p.c, p.set_z(t - 1, p.s)), (1 - p.c, p.set_z(t - 1, -p.s)))

        @pl.when(odd)
        def _():
            g.z_b(t)

            @pl.when(t + 1 < NSETS)
            def _():
                g.z_b(t + 1)

        bufs = (s_a, s_b)
        top = scores(0, bufs[0], parts)
        for i in range(6):
            following = scores(i + 1, bufs[(i + 1) % 2], parts) if i < 5 else None
            weigh(i, bufs[i % 2], top, parts)
            top = following
            if i == 0:
                @pl.when(jnp.logical_not(last))
                def _():
                    g.x1(t)
            if i == 1:
                @pl.when(odd)
                def _():
                    g.z_a(t)

                    @pl.when(t + 1 < NSETS)
                    def _():
                        g.z_a(t + 1)
            if i == 2:
                @pl.when(jnp.logical_not(last))
                def _():
                    g.x2(t)
            if i == 3:
                @pl.when(jnp.logical_not(last))
                def _():
                    g.x3(t)
            if i == 5:
                @pl.when(jnp.logical_not(last))
                def _():
                    g.arrived(t)

    w.start_b()
    w.start_a()

    o_a = [acc_a[h, 0:64, :] / acc_a[h, 64:65, :] for h in range(4)]
    attn[:, 0:256] = jnp.concatenate(o_a, axis=0).T.astype(BF16)
    o_b = [acc_b[h, 0:128, :] / acc_b[h, 128:129, :] for h in range(2)]
    attn[:, 256:512] = jnp.concatenate(o_b, axis=0).T.astype(BF16)
    own_oa.wait()
    own_ob.wait()
    for k in range(8):
        cols = slice(k * 256, k * 256 + 256)
        tile = dot(attn[:, 0:256], woa[:, cols]) + dot(attn[:, 256:512], wob[:, cols])
        part[:, k // 4, :, (k % 4) * 256:(k % 4) * 256 + 256] = tile.astype(BF16).reshape(4, 64, 256)

    def to_y(src, dst, s_sem, r_sem, y):
        return pltpu.make_async_remote_copy(src_ref=src, dst_ref=dst, send_sem=s_sem, recv_sem=r_sem,
                                            device_id={"tp": y}, device_id_type=MESH)

    def reduce_copies(src, mids, ins, ss, rr):
        return (
            to_y(src.at[opp, 0], mids.at[0], ss.at[0], rr.at[0], up),
            to_y(src.at[opp, 1], mids.at[1], ss.at[1], rr.at[1], down),
            to_y(src.at[down, 0], ins.at[0], ss.at[2], rr.at[2], down),
            to_y(src.at[up, 1], ins.at[1], ss.at[3], rr.at[3], up),
            to_y(mids.at[2], ins.at[2], ss.at[4], rr.at[4], up),
            to_y(mids.at[3], ins.at[3], ss.at[5], rr.at[5], down),
        )

    def reduce_first(copies):
        for copy in copies[:4]:
            copy.start()

    def reduce_second(copies, src, mids):
        copies[0].wait_recv()
        mids[2] = (src[up, 0].astype(F32) + mids[0].astype(F32)).astype(BF16)
        copies[1].wait_recv()
        mids[3] = (src[down, 1].astype(F32) + mids[1].astype(F32)).astype(BF16)
        copies[4].start()
        copies[5].start()

    def reduce_last(copies):
        for copy in copies[2:]:
            copy.wait_recv()

    first = reduce_copies(part, rs_mid, rs_in, rs_s, rs_r)
    reduce_first(first)
    w.x_a()
    reduce_second(first, part, rs_mid)
    w.x1(0)
    w.x2(0)
    w.x3(0)
    w.arrived(0)
    reduce_last(first)

    def own_sum(src, ins, h):
        mine = src[p.y, h].astype(F32)
        from_up, from_down = (0, 2) if h == 0 else (3, 1)
        return mine + ins[from_up].astype(F32) + ins[from_down].astype(F32)

    square = None
    for h in range(2):
        cols = slice(h * 1024, h * 1024 + 1024)
        m = x_ref[:, cols].astype(F32) + own_sum(part, rs_in, h)
        mid[:, cols] = m
        sq = jnp.sum(m * m, axis=1, keepdims=True)
        square = sq if square is None else square + sq
    inv = lax.rsqrt(square * (1.0 / 2048) + norm_eps)
    for h in range(2):
        cols = slice(h * 1024, h * 1024 + 1024)
        ag[p.y, h] = (mid[:, cols] * inv * gain_ref[:, cols]).astype(BF16)

    def ag_copy(k, d, h, y):
        return to_y(ag.at[d, h], ag.at[d, h], ag_s.at[k], ag_r.at[k], y)

    gathers = (
        ag_copy(0, p.y, 0, up), ag_copy(1, p.y, 1, down), ag_copy(2, p.y, 1, up), ag_copy(3, p.y, 0, down),
        ag_copy(4, down, 0, up), ag_copy(5, up, 1, down),
    )
    for copy in gathers[:4]:
        copy.start()

    def weights_pair(t):
        w.z_b(t)
        if t + 1 < NSETS:
            w.z_b(t + 1)
        w.z_a(t)
        if t + 1 < NSETS:
            w.z_a(t + 1)
        for u in (t, t + 1):
            if u < NSETS:
                w.x1(u)
                w.x2(u)
                w.x3(u)
                w.arrived(u)

    weights_pair(1)
    gathers[0].wait_recv()
    gathers[4].start()
    gathers[1].wait_recv()
    gathers[5].start()
    for t in (3, 5, 7):
        weights_pair(t)
    for copy in gathers[2:]:
        copy.wait_recv()

    rows = [ag[:, h].reshape(256, 1024) for h in range(2)]
    for m in range(2):
        for k in range(3):
            cols = slice(k * 256, k * 256 + 256)
            tile = None
            for h in range(2):
                block = wgu[16 * h:16 * h + 16, :, m, :, cols].reshape(1024, 256)
                o = dot(rows[h], block)
                tile = o if tile is None else tile + o
            pre[:, m * 768 + k * 256:m * 768 + k * 256 + 256] = tile.astype(BF16)

    def halo_copy(k, src, sp):
        return pltpu.make_async_remote_copy(src_ref=src, dst_ref=halo.at[k], send_sem=h_s.at[k], recv_sem=h_r.at[k],
                                            device_id={"sp": sp}, device_id_type=MESH)

    halos = (halo_copy(0, pre.at[240:256, :], sp_next), halo_copy(1, pre.at[0:16, :], sp_prev))
    for copy in halos:
        copy.start()
    for copy in halos:
        copy.wait_recv()
    keep_prev = jnp.where(p.sp == 0, 0.0, 1.0).astype(F32)
    keep_next = jnp.where(p.sp == 63, 0.0, 1.0).astype(F32)
    row = lax.broadcasted_iota(jnp.int32, (256, 256), 0)
    for k in range(3):
        mixed = []
        for m, taps in ((0, cg_ref), (1, cu_ref)):
            cols = slice(m * 768 + k * 256, m * 768 + k * 256 + 256)
            tcols = slice(k * 256, k * 256 + 256)
            now = pre[:, cols].astype(F32)
            before = halo[0, :, cols].astype(F32)[15:16, :] * keep_prev
            after = halo[1, :, cols].astype(F32)[0:1, :] * keep_next
            prev = jnp.where(row == 0, before, pltpu.roll(now, 1, 0))
            nxt = jnp.where(row == 255, after, pltpu.roll(now, 255, 0))
            mixed.append(prev * taps[0:1, tcols] + now * taps[1:2, tcols] + nxt * taps[2:3, tcols])
        gate, upv = mixed
        hid[:, k * 256:k * 256 + 256] = (gate / (1.0 + jnp.exp(-gate)) * upv).astype(BF16)

    for k in range(8):
        block = wd[4 * k:4 * k + 4].reshape(256, 768)
        tile = lax.dot_general(hid[...], block, (((1,), (1,)), ((), ())), preferred_element_type=F32)
        part2[:, k // 4, :, (k % 4) * 256:(k % 4) * 256 + 256] = tile.astype(BF16).reshape(4, 64, 256)

    second = reduce_copies(part2, rs_mid2, rs_in2, rs_s2, rs_r2)
    reduce_first(second)
    g.drain()
    w.drain()
    reduce_second(second, part2, rs_mid2)
    reduce_last(second)
    for h in range(2):
        cols = slice(h * 1024, h * 1024 + 1024)
        out_ref[:, cols] = (mid[:, cols] + own_sum(part2, rs_in2, h)).astype(BF16)
    for copy in (*first, *second, *gathers, *halos):
        copy.wait_send()


def fused(*args):
    vm = pl.BlockSpec(memory_space=pltpu.VMEM)
    hb = pl.BlockSpec(memory_space=pltpu.HBM)
    v, d = pltpu.VMEM, pltpu.SemaphoreType.DMA
    scratch = [
        v((2, NZ, NX, 256, 128), BF16), v((2, NZ, NX, 512, 128), BF16),
        v((32, 2, 2, 32, 768), BF16), v((32, 2, 32, 768), BF16),
        v((256, 2048), BF16), v((256, 2048), BF16),
        v((2048, 256), F32), v((2048, 256), F32), v((2048, 256), BF16),
        v((4, 80, 256), F32), v((2, 144, 256), F32), v((6, 1, 256), F32),
        v((256, 512), BF16), v((4, 2, 64, 1024), BF16), v((4, 64, 1024), BF16), v((4, 64, 1024), BF16),
        v((64, 2048), F32), v((4, 2, 64, 1024), BF16), v((256, 1536), BF16), v((2, 16, 1536), BF16),
        v((256, 768), BF16), v((4, 2, 64, 1024), BF16), v((4, 64, 1024), BF16), v((4, 64, 1024), BF16),
        d((4,)), d((2,)), d((6,)), d((6,)), d((6,)), d((6,)), d((6,)), d((6,)), d((2,)), d((2,)),
        *gather_sems(), *gather_sems(),
    ]
    return pl.pallas_call(
        kernel,
        out_shape=jax.ShapeDtypeStruct((64, 2048), BF16),
        in_specs=[hb, hb, vm, vm, hb, hb, hb, hb, vm, vm, vm, vm],
        out_specs=vm,
        scratch_shapes=scratch,
        compiler_params=pltpu.CompilerParams(
            collective_id=0, has_side_effects=True, vmem_limit_bytes=60 * 1024 * 1024
        ),
        name="layer",
    )(*args)


def on_device(
    x_res, q_a, k_a, v_a, q_b, k_b, v_b, gain_qa, gain_ka, gain_qb, gain_kb,
    w_out_a, w_out_b, gain_mid, w_gate, w_up, conv_gate, conv_up, w_down,
):
    rows = q_a.shape[0]
    positions = lax.axis_index("sp") * rows + lax.iota(jnp.int32, rows)
    qa = prepare(q_a, gain_qa, DHA, positions)
    qb = prepare(q_b, gain_qb, DHB, positions)
    ka = prepare(k_a, gain_ka, DHA, positions)[:, 0]
    kb = prepare(k_b, gain_kb, DHB, positions)[:, 0]
    qa_t = jnp.transpose(qa * BF16(0.125), (1, 2, 0))
    qb_t = jnp.transpose(qb, (1, 2, 0))
    ka2 = jnp.concatenate([ka[:128], ka[128:]], axis=1)
    kva = jnp.concatenate([ka2, v_a[:128].T, v_a[128:].T], axis=0)
    kvb = jnp.concatenate([kb, v_b[:128].T, v_b[128:].T], axis=0)
    wgu = jnp.stack([w_gate, w_up])
    return fused(kva, kvb, qa_t, qb_t, wgu, w_down.T, w_out_a, w_out_b, x_res, gain_mid[None, :], conv_gate, conv_up)


def solution(mesh):
    in_specs = (
        P(("sp", "tp"), None), P("sp", "tp"), P("sp", "tp"), P("sp", "tp"), P("sp", "tp"), P("sp", "tp"), P("sp", "tp"),
        P(), P(), P(), P(), P("tp", None), P("tp", None), P(),
        P("sp", "tp"), P("sp", "tp"), P(None, "tp"), P(None, "tp"), P("tp", "sp"),
    )
    return jax.shard_map(
        on_device, mesh=mesh, in_specs=in_specs, out_specs=P(("sp", "tp"), None), check_vma=False
    )
```

time: 371 us -> 185 us (0.50)
  matrix products: 170 us -> 0 us
  Pallas kernels: 0 us -> 169 us
  waiting for transfers between devices: 91.8 us -> 0 us
  blocking collectives: 35.3 us -> 0 us
  other arithmetic: 28.9 us -> 6.14 us
  between operations: 13.7 us -> 0.28 us
  starting transfers between devices: 10.5 us -> 0 us
  local copies, waits for them, and re-layouts: 16.6 us -> 9.21 us
    dot_general x69 -> x0, matrix products: 170 us -> none  [the longest x32 80.8 us: one_span(): jnp.einsum('qkgd,skd->kgqs', queries, key_rows, preferred_element_type=jn...]
    pallas_call x0 -> x1, Pallas kernels: none -> 169 us  [fused(): pl.pallas_call(kernel, out_shape=jax.ShapeDtypeStruct((64, 2048), BF16),...]
    all_gather x3 -> x0, waiting for transfers between devices: 74.8 us -> none  [the longest x2 74.8 us: side_by_side(): result = lax.all_gather(both, axis, axis=dim, tiled=True)]
    all_to_all x2 -> x0, blocking collectives: 35.3 us -> none  [sent_and_summed(): lax.all_to_all(parts, axis, split_axis=0, concat_axis=0, tiled=True)]
    reduce_sum x35 -> x0, other arithmetic: 17.6 us -> none  [the longest x32 17.1 us: one_span(): totals = totals * factor + jnp.sum(expd, axis=-1)]
    all_to_all x1 -> x0, waiting for transfers between devices: 14 us -> none  [sent_to_all(): return lax.all_to_all(copies, axis, split_axis=0, concat_axis=0, tiled=True)]
    reshape x2, local copies, waits for them, and re-layouts: 10.5 us -> 0.19 us  [prepare(): values = raw.astype(jnp.float32).reshape(count, heads, head_size)]
    unnamed x33 -> x26, local copies, waits for them, and re-layouts: 0.3 us -> 8.65 us
  transfers between devices with their start and end apart: 6 -> 0, of which waited for: 3 -> 0; matrix products, arithmetic and copies ran while one was open for 54% -> 0% of each run, Pallas kernels for 0% -> 0%
where the time goes in v1:
time: 185 us
  Pallas kernels  169 us (91%)
  local copies, waits for them, and re-layouts  9.21 us (5%)
  other arithmetic  6.14 us (3%)
    pallas_call x1, Pallas kernels, fused(): pl.pallas_call(kernel, out_shape=jax.ShapeDtypeStruct((64, 2048), BF16),...  169 us
    unnamed x26, local copies, waits for them, and re-layouts  8.65 us

profile of v1, /device:TPU:1, one launch (start us, length us, event | category | flops | bytes accessed | tf_op | source)
XLA Modules:
  0.0 184.7 jit_solution(13571827839509321347)
XLA Ops:
  0.0 0.9 copy.20
  1.0 0.6 copy-done.7
  1.8 0.2 fusion.19
  2.0 0.1 broadcast_multiply_fusion.3
  2.1 0.6 fusion.9
  2.9 0.8 copy-done.1
  3.9 0.6 copy-done.10
  4.7 0.8 multiply_bitcast_fusion.qa_ref
  5.4 0.8 copy-done.6
  6.2 0.7 pad_maximum_fusion.4.kva_h
  6.9 0.1 broadcast_multiply_fusion.1
  7.0 0.7 copy-done
  7.9 0.6 copy-done.8
  8.6 0.2 fusion.17
  8.8 0.6 fusion.15
  9.7 0.8 copy-done.2
  10.6 0.6 copy-done.9
  11.4 0.7 fusion.20.qb_ref
  12.3 0.1 copy.30
  12.5 0.7 pad_maximum_fusion.2.kvb_h
  13.1 0.1 copy-done.4
  13.3 0.6 pad_maximum_fusion.3.wgu_h
  14.0 169.0 %layer.1 = bf16[64,2048]{1,0:T(8,128)(2,1)} custom-call(bf16[256,128]{1,0:T(8,128)(2,1)} %pad_maximum_fusion.4.kva_h, bf16[512,128]{1,0:T(8,128)(2,1)} %pad_maximum_fusion.2.kvb_h, bf16[4,64,256]{2,1,0:T(8,128)(2,1)} %multiply_bitcast_fusion.qa_ref, bf16[2,128,256]{2,1,0:T(8,128)(2,1)} %fusion.20.qb_ref, bf16[2,32,768]{2,1,0:T(8,128)(2,1)} %pad_maximum_fusion.3.wgu_h, ...), custom_call_target="tpu_custom_call" | custom-call | tf_op jit(solution)/shard_map/layer/pallas_call | solution.py:525
  183.0 1.7 copy.32
  (40 shorter events, 1.6 us)
Async XLA Ops:
  1.0 0.7 copy-start.7
  2.8 0.9 copy-start.1
  3.9 0.7 copy-start.10
  5.4 0.8 copy-start.6
  6.9 0.8 copy-start
  7.9 0.7 copy-start.8
  9.5 0.9 copy-start.2
  10.6 0.7 copy-start.9
  11.4 0.8 copy-start.3
  12.5 0.8 copy-start.4
  12.5 0.8 copy-start.5

commit v2 on v1

--- a/solution.py
+++ b/solution.py
@@ -3,6 +3,7 @@
 
 import jax
 import jax.numpy as jnp
+import numpy as np
 from jax import lax
 from jax.experimental import pallas as pl
 from jax.experimental.pallas import tpu as pltpu
@@ -23,31 +24,18 @@
 rope_theta = 10000.0
 
 
-def rotary_angles(positions, head_size):
+def rotary_tables(head_size):
     half = head_size // 2
-    inverse = jnp.power(jnp.float32(rope_theta), -jnp.arange(0, half, 2, dtype=jnp.float32) / half)
-    grid_row = (positions // 64).astype(jnp.float32)[:, None] * inverse[None, :]
-    grid_col = (positions % 64).astype(jnp.float32)[:, None] * inverse[None, :]
-    angles = jnp.concatenate([grid_row, grid_row, grid_col, grid_col], axis=-1)
-    return (jnp.cos(angles), jnp.sin(angles))
-
-
-def rotate_half(values):
-    first, second = jnp.split(values, 2, axis=-1)
-    return jnp.concatenate([-second, first], axis=-1)
-
-
-def prepare(raw, gain, head_size, positions):
-    count = raw.shape[0]
-    heads = raw.shape[1] // head_size
-    values = raw.astype(jnp.float32).reshape(count, heads, head_size)
-    values = values * lax.rsqrt(jnp.mean(values * values, axis=-1, keepdims=True) + norm_eps)
-    values = values * gain
-    cosine, sine = rotary_angles(positions, head_size)
-    row_part, col_part = jnp.split(values, 2, axis=-1)
-    turned = jnp.concatenate([rotate_half(row_part), rotate_half(col_part)], axis=-1)
-    values = values * cosine[:, None, :] + turned * sine[:, None, :]
-    return values.astype(jnp.bfloat16)
+    quarter = head_size // 4
+    inverse = np.power(np.float32(rope_theta), -np.arange(0, half, 2, dtype=np.float32) / np.float32(half)).astype(np.float32)
+    lane = np.arange(128)
+    per_lane = inverse[lane % quarter]
+    sign = np.where(lane % half < quarter, -1.0, 1.0)
+    angle_r = (np.arange(256, dtype=np.float32)[:, None] * per_lane[None, :]).astype(np.float64)
+    rows = np.concatenate([np.cos(angle_r).reshape(64, 4, 128), (np.sin(angle_r) * sign).reshape(64, 4, 128)], axis=1)
+    angle_c = angle_r[:64]
+    cols = np.stack([np.cos(angle_c), np.sin(angle_c) * sign])
+    return rows.astype(np.float32), cols.astype(np.float32)
 
 
 class Place:
@@ -206,10 +194,10 @@
     return jnp.dot(a, b, preferred_element_type=F32)
 
 
-def kernel(kva_h, kvb_h, qa_ref, qb_ref, wgu_h, wd_h, woa_h, wob_h, x_ref, gain_ref, cg_ref, cu_ref, out_ref,
-           ba, bb, wgu, wd, woa, wob, s_a, s_b, p_ref, acc_a, acc_b, mx,
+def kernel(q_a, k_a, v_a, q_b, k_b, v_b, ra_h, rb_h, col_a, col_b, g_qa, g_ka, g_qb, g_kb, wg_h, wu_h, wd_h, woa_h, wob_h, x_ref, gain_ref, cg_ref, cu_ref, out_ref,
+           qa_in, ka_in, va_in, qb_in, kb_in, vb_in, ra, rb, qa_ref, qb_ref, ba, bb, wa, wb, woa, wob, s_a, s_b, p_ref, acc_a, acc_b, mx,
            attn, part, rs_mid, rs_in, mid, ag, pre, halo, hid, part2, rs_mid2, rs_in2,
-           loc, wo_sem, rs_s, rs_r, rs_s2, rs_r2, ag_s, ag_r, h_s, h_r, *sems):
+           in_sem, loc, wo_sem, rs_s, rs_r, rs_s2, rs_r2, ag_s, ag_r, h_s, h_r, *sems):
     p = Place()
     n = len(sems) // 2
 
@@ -217,13 +205,19 @@
     up, down = (p.y + 1) % NY, (p.y + NY - 1) % NY
     opp = (p.y + 2) % NY
     sp_next, sp_prev = (p.sp + 1) % 64, (p.sp + 63) % 64
-    own_a = pltpu.make_async_copy(kva_h, ba.at[p.c, p.z, p.x], loc.at[0])
-    own_b = pltpu.make_async_copy(kvb_h, bb.at[p.c, p.z, p.x], loc.at[1])
-    own_gu = pltpu.make_async_copy(wgu_h, wgu.at[p.z * NX + p.x, p.c], loc.at[2])
-    own_d = pltpu.make_async_copy(wd_h, wd.at[p.z * NX + p.x, p.c], loc.at[3])
+    pairs = ((k_a, ka_in), (v_a, va_in), (k_b, kb_in), (v_b, vb_in), (ra_h.at[p.sp], ra), (rb_h.at[p.sp], rb),
+             (q_a, qa_in), (q_b, qb_in))
+    inputs = [pltpu.make_async_copy(src, dst, in_sem.at[i]) for i, (src, dst) in enumerate(pairs)]
+    for copy in inputs:
+        copy.start()
+    zx = p.z * NX + p.x
+    own_g = pltpu.make_async_copy(wg_h, wa.at[zx, p.c, :, pl.ds(0, 768)], loc.at[0])
+    own_ua = pltpu.make_async_copy(wu_h.at[:, pl.ds(0, 384)], wa.at[zx, p.c, :, pl.ds(768, 384)], loc.at[1])
+    own_ub = pltpu.make_async_copy(wu_h.at[:, pl.ds(384, 384)], wb.at[zx, p.c, :, pl.ds(0, 384)], loc.at[2])
+    own_d = pltpu.make_async_copy(wd_h, wb.at[zx, p.c, :, pl.ds(384, 768)], loc.at[3])
     own_oa = pltpu.make_async_copy(woa_h, woa, wo_sem.at[0])
     own_ob = pltpu.make_async_copy(wob_h, wob, wo_sem.at[1])
-    for copy in (own_b, own_a, own_gu, own_d, own_oa, own_ob):
+    for copy in (own_g, own_ua, own_ub, own_d, own_oa, own_ob):
         copy.start()
     greeted = [p.at(p.zz(1), p.x, p.c), p.at(p.zz(-1), p.x, p.c), p.at(p.z, p.xx(1), p.c), p.at(p.z, p.xx(-1), p.c),
                p.at(p.z, p.x, 1 - p.c), sp_next, sp_prev]
@@ -231,26 +225,90 @@
         pl.semaphore_signal(barrier, inc=1, device_id={"sp": sp}, device_id_type=MESH)
     for y in (up, down):
         pl.semaphore_signal(barrier, inc=1, device_id={"tp": y}, device_id_type=MESH)
+
+    lane = lax.broadcasted_iota(jnp.int32, (64, 128), 1)
+    first_head = lane < 64
+
+    def normed_a(v, gain):
+        sq = v * v
+        left = jnp.sum(jnp.where(first_head, sq, 0.0), axis=1, keepdims=True)
+        right = jnp.sum(jnp.where(first_head, 0.0, sq), axis=1, keepdims=True)
+        inv = lax.rsqrt(jnp.where(first_head, left, right) * (1.0 / DHA) + norm_eps)
+        gains = jnp.concatenate([gain[...], gain[...]], axis=1)
+        return v * inv * gains
+
+    def normed_b(v, gain):
+        inv = lax.rsqrt(jnp.sum(v * v, axis=1, keepdims=True) * (1.0 / DHB) + norm_eps)
+        return v * inv * gain[...]
+
+    def turned(v, quarter, cos, sin):
+        other = jnp.where(lane % (2 * quarter) < quarter, pltpu.roll(v, 128 - quarter, 1), pltpu.roll(v, quarter, 1))
+        return v * cos + other * sin
+
+    def turned_a(v, left, right):
+        row_lane = lane % 64 < 32
+
+        def table(k):
+            row = jnp.where(first_head, ra[4 * k + left:4 * k + left + 1, :], ra[4 * k + right:4 * k + right + 1, :])
+            return jnp.where(row_lane, row, col_a[k])
+
+        return turned(v, 16, table(0), table(1))
+
+    def turned_b(v, block):
+        def table(k):
+            return jnp.where(first_head, rb[4 * k + block:4 * k + block + 1, :], col_b[k])
+
+        return turned(v, 32, table(0), table(1))
+
+    for copy in inputs[:6]:
+        copy.wait()
+    slot_a, slot_b = ba.at[p.c, p.z, p.x], bb.at[p.c, p.z, p.x]
+    ka = ka_in[...].astype(F32).T
+    for k in range(2):
+        v = jnp.concatenate([ka[64 * k:64 * k + 64, :], ka[128 + 64 * k:192 + 64 * k, :]], axis=1)
+        slot_a[64 * k:64 * k + 64, :] = turned_a(normed_a(v, g_ka), k, k + 2).astype(BF16)
+    slot_a[128:192, :] = va_in[:, 0:128]
+    slot_a[192:256, :] = va_in[:, 128:256]
+    for k in range(4):
+        v = kb_in[64 * k:64 * k + 64, :].astype(F32)
+        slot_b[64 * k:64 * k + 64, :] = turned_b(normed_b(v, g_kb), k).astype(BF16)
+    vt = vb_in[...].astype(F32).T.astype(BF16)
+    slot_b[256:384, :] = vt[:, 0:128]
+    slot_b[384:512, :] = vt[:, 128:256]
     pl.semaphore_wait(barrier, 9)
 
     g = Gather(p, lambda z, c: ba.at[c, z], lambda z, x, c: ba.at[c, z, x], lambda z, x, c: bb.at[c, z, x], sems[:n])
-    w = Gather(p, lambda z, c: wgu.at[pl.ds(z * NX, NX), c], lambda z, x, c: wgu.at[z * NX + x, c],
-               lambda z, x, c: wd.at[z * NX + x, c], sems[n:])
-
-    own_b.wait()
+    w = Gather(p, lambda z, c: wa.at[pl.ds(z * NX, NX), c], lambda z, x, c: wa.at[z * NX + x, c],
+               lambda z, x, c: wb.at[z * NX + x, c], sems[n:])
+
+    g.start_a()
     g.start_b()
-    own_a.wait()
-    g.start_a()
-    own_gu.wait()
-    own_d.wait()
+    inputs[6].wait()
+    inputs[7].wait()
+    for h in range(2):
+        blocks = []
+        for k in range(4):
+            v = qa_in[64 * k:64 * k + 64, 128 * h:128 * h + 128].astype(F32)
+            blocks.append(turned_a(normed_a(v, g_qa), k, k) * 0.125)
+        qt = jnp.concatenate(blocks, axis=0).T.astype(BF16)
+        qa_ref[2 * h] = qt[0:64, :]
+        qa_ref[2 * h + 1] = qt[64:128, :]
+    for h in range(2):
+        blocks = []
+        for k in range(4):
+            v = qb_in[64 * k:64 * k + 64, 128 * h:128 * h + 128].astype(F32)
+            blocks.append(turned_b(normed_b(v, g_qb), k))
+        qb_ref[h] = jnp.concatenate(blocks, axis=0).T.astype(BF16)
     acc_a[...] = jnp.zeros_like(acc_a)
     acc_b[...] = jnp.zeros_like(acc_b)
     mx[...] = jnp.full_like(mx, -1e30)
     g.x_a()
+    for copy in (own_g, own_ua, own_ub, own_d):
+        copy.wait()
     g.x1(0)
     g.x2(0)
-    g.x3(0)
-    g.arrived(0)
+    g.z_b(1)
+    g.z_b(2)
 
     zeros64 = jnp.zeros((64, 256), BF16)
 
@@ -303,17 +361,15 @@
 
     @pl.loop(1, NSETS + 1)
     def _(t):
-        last = t == NSETS
         odd = t % 2 == 1
         parts = ((p.c, p.set_z(t - 1, p.s)), (1 - p.c, p.set_z(t - 1, -p.s)))
+        g.x3(t - 1)
+        g.arrived(t - 1)
 
         @pl.when(odd)
         def _():
-            g.z_b(t)
-
-            @pl.when(t + 1 < NSETS)
-            def _():
-                g.z_b(t + 1)
+            g.x1(t)
+            g.x2(t)
 
         bufs = (s_a, s_b)
         top = scores(0, bufs[0], parts)
@@ -321,10 +377,6 @@
             following = scores(i + 1, bufs[(i + 1) % 2], parts) if i < 5 else None
             weigh(i, bufs[i % 2], top, parts)
             top = following
-            if i == 0:
-                @pl.when(jnp.logical_not(last))
-                def _():
-                    g.x1(t)
             if i == 1:
                 @pl.when(odd)
                 def _():
@@ -333,21 +385,45 @@
                     @pl.when(t + 1 < NSETS)
                     def _():
                         g.z_a(t + 1)
-            if i == 2:
-                @pl.when(jnp.logical_not(last))
+
+                @pl.when(t == 4)
                 def _():
-                    g.x2(t)
+                    w.start_a()
+                    w.start_b()
             if i == 3:
-                @pl.when(jnp.logical_not(last))
+                @pl.when(jnp.logical_and(odd, t + 1 < NSETS))
                 def _():
-                    g.x3(t)
+                    g.x1(t + 1)
+                    g.x2(t + 1)
+
+                @pl.when(t == 6)
+                def _():
+                    w.x_a()
+                    w.x1(0)
             if i == 5:
-                @pl.when(jnp.logical_not(last))
+                @pl.when(jnp.logical_and(odd, t + 2 < NSETS))
                 def _():
-                    g.arrived(t)
-
-    w.start_b()
-    w.start_a()
+                    g.z_b(t + 2)
+
+                    @pl.when(t + 3 < NSETS)
+                    def _():
+                        g.z_b(t + 3)
+
+    def w_b(t):
+        for u in (t, t + 1):
+            if u < NSETS:
+                w.z_b(u)
+
+    def w_a(t):
+        for u in (t, t + 1):
+            if u < NSETS:
+                w.z_a(u)
+
+    def w_x(t):
+        for u in (t, t + 1):
+            if u < NSETS:
+                w.x1(u)
+
 
     o_a = [acc_a[h, 0:64, :] / acc_a[h, 64:65, :] for h in range(4)]
     attn[:, 0:256] = jnp.concatenate(o_a, axis=0).T.astype(BF16)
@@ -392,12 +468,11 @@
 
     first = reduce_copies(part, rs_mid, rs_in, rs_s, rs_r)
     reduce_first(first)
-    w.x_a()
+    w_b(1)
+    w_a(1)
+    w_x(1)
     reduce_second(first, part, rs_mid)
-    w.x1(0)
-    w.x2(0)
-    w.x3(0)
-    w.arrived(0)
+    w_b(3)
     reduce_last(first)
 
     def own_sum(src, ins, h):
@@ -427,27 +502,26 @@
     for copy in gathers[:4]:
         copy.start()
 
-    def weights_pair(t):
-        w.z_b(t)
-        if t + 1 < NSETS:
-            w.z_b(t + 1)
-        w.z_a(t)
-        if t + 1 < NSETS:
-            w.z_a(t + 1)
-        for u in (t, t + 1):
-            if u < NSETS:
-                w.x1(u)
-                w.x2(u)
-                w.x3(u)
-                w.arrived(u)
-
-    weights_pair(1)
+    w_a(3)
+    w_x(3)
     gathers[0].wait_recv()
     gathers[4].start()
     gathers[1].wait_recv()
     gathers[5].start()
-    for t in (3, 5, 7):
-        weights_pair(t)
+    for t in (5, 7):
+        w_b(t)
+        w_a(t)
+        w_x(t)
+
+    @pl.loop(0, NSETS)
+    def _(t):
+        w.x2(t)
+        w.x3(t)
+
+    @pl.loop(0, NSETS)
+    def _(t):
+        w.arrived(t)
+
     for copy in gathers[2:]:
         copy.wait_recv()
 
@@ -457,7 +531,16 @@
             cols = slice(k * 256, k * 256 + 256)
             tile = None
             for h in range(2):
-                block = wgu[16 * h:16 * h + 16, :, m, :, cols].reshape(1024, 256)
+                half = slice(16 * h, 16 * h + 16)
+                if m == 0:
+                    block = wa[half, :, :, cols]
+                elif k == 0:
+                    block = wa[half, :, :, 768:1024]
+                elif k == 1:
+                    block = jnp.concatenate([wa[half, :, :, 1024:1152], wb[half, :, :, 0:128]], axis=-1)
+                else:
+                    block = wb[half, :, :, 128:384]
+                block = block.reshape(1024, 256)
                 o = dot(rows[h], block)
                 tile = o if tile is None else tile + o
             pre[:, m * 768 + k * 256:m * 768 + k * 256 + 256] = tile.astype(BF16)
@@ -489,7 +572,7 @@
         hid[:, k * 256:k * 256 + 256] = (gate / (1.0 + jnp.exp(-gate)) * upv).astype(BF16)
 
     for k in range(8):
-        block = wd[4 * k:4 * k + 4].reshape(256, 768)
+        block = wb[4 * k:4 * k + 4, :, :, 384:1152].reshape(256, 768)
         tile = lax.dot_general(hid[...], block, (((1,), (1,)), ((), ())), preferred_element_type=F32)
         part2[:, k // 4, :, (k % 4) * 256:(k % 4) * 256 + 256] = tile.astype(BF16).reshape(4, 64, 256)
 
@@ -511,21 +594,24 @@
     hb = pl.BlockSpec(memory_space=pltpu.HBM)
     v, d = pltpu.VMEM, pltpu.SemaphoreType.DMA
     scratch = [
+        v((256, 256), BF16), v((64, 256), BF16), v((64, 256), BF16), v((256, 256), BF16), v((256, 128), BF16),
+        v((256, 128), BF16), v((8, 128), F32), v((8, 128), F32),
+        v((4, 64, 256), BF16), v((2, 128, 256), BF16),
         v((2, NZ, NX, 256, 128), BF16), v((2, NZ, NX, 512, 128), BF16),
-        v((32, 2, 2, 32, 768), BF16), v((32, 2, 32, 768), BF16),
+        v((32, 2, 32, 1152), BF16), v((32, 2, 32, 1152), BF16),
         v((256, 2048), BF16), v((256, 2048), BF16),
         v((2048, 256), F32), v((2048, 256), F32), v((2048, 256), BF16),
         v((4, 80, 256), F32), v((2, 144, 256), F32), v((6, 1, 256), F32),
         v((256, 512), BF16), v((4, 2, 64, 1024), BF16), v((4, 64, 1024), BF16), v((4, 64, 1024), BF16),
         v((64, 2048), F32), v((4, 2, 64, 1024), BF16), v((256, 1536), BF16), v((2, 16, 1536), BF16),
         v((256, 768), BF16), v((4, 2, 64, 1024), BF16), v((4, 64, 1024), BF16), v((4, 64, 1024), BF16),
-        d((4,)), d((2,)), d((6,)), d((6,)), d((6,)), d((6,)), d((6,)), d((6,)), d((2,)), d((2,)),
+        d((8,)), d((4,)), d((2,)), d((6,)), d((6,)), d((6,)), d((6,)), d((6,)), d((6,)), d((2,)), d((2,)),
         *gather_sems(), *gather_sems(),
     ]
     return pl.pallas_call(
         kernel,
         out_shape=jax.ShapeDtypeStruct((64, 2048), BF16),
-        in_specs=[hb, hb, vm, vm, hb, hb, hb, hb, vm, vm, vm, vm],
+        in_specs=[hb] * 8 + [vm] * 6 + [hb] * 5 + [vm] * 4,
         out_specs=vm,
         scratch_shapes=scratch,
         compiler_params=pltpu.CompilerParams(
@@ -539,19 +625,13 @@
     x_res, q_a, k_a, v_a, q_b, k_b, v_b, gain_qa, gain_ka, gain_qb, gain_kb,
     w_out_a, w_out_b, gain_mid, w_gate, w_up, conv_gate, conv_up, w_down,
 ):
-    rows = q_a.shape[0]
-    positions = lax.axis_index("sp") * rows + lax.iota(jnp.int32, rows)
-    qa = prepare(q_a, gain_qa, DHA, positions)
-    qb = prepare(q_b, gain_qb, DHB, positions)
-    ka = prepare(k_a, gain_ka, DHA, positions)[:, 0]
-    kb = prepare(k_b, gain_kb, DHB, positions)[:, 0]
-    qa_t = jnp.transpose(qa * BF16(0.125), (1, 2, 0))
-    qb_t = jnp.transpose(qb, (1, 2, 0))
-    ka2 = jnp.concatenate([ka[:128], ka[128:]], axis=1)
-    kva = jnp.concatenate([ka2, v_a[:128].T, v_a[128:].T], axis=0)
-    kvb = jnp.concatenate([kb, v_b[:128].T, v_b[128:].T], axis=0)
-    wgu = jnp.stack([w_gate, w_up])
-    return fused(kva, kvb, qa_t, qb_t, wgu, w_down.T, w_out_a, w_out_b, x_res, gain_mid[None, :], conv_gate, conv_up)
+    rows_a, cols_a = rotary_tables(DHA)
+    rows_b, cols_b = rotary_tables(DHB)
+    return fused(
+        q_a, k_a.T, v_a.T, q_b, k_b, v_b, rows_a, rows_b, cols_a, cols_b,
+        gain_qa[None, :], gain_ka[None, :], gain_qb[None, :], gain_kb[None, :],
+        w_gate, w_up, w_down.T, w_out_a, w_out_b, x_res, gain_mid[None, :], conv_gate, conv_up,
+    )
 
 
 def solution(mesh):

time: 185 us -> 128 us (0.69)
  Pallas kernels: 169 us -> 125 us
  local copies, waits for them, and re-layouts: 9.21 us -> 1.67 us
  other arithmetic: 6.14 us -> 0 us
    pallas_call x1, Pallas kernels: 169 us -> 125 us  [fused(): pl.pallas_call(kernel, out_shape=jax.ShapeDtypeStruct((64, 2048), BF16),...]
    unnamed x26 -> x1, local copies, waits for them, and re-layouts: 8.65 us -> 1.67 us
where the time goes in v2:
time: 128 us; the launch traced here: 127 us
  Pallas kernels  125 us (98%)
  local copies, waits for them, and re-layouts  1.67 us (1%)
    pallas_call x1, Pallas kernels, fused(): pl.pallas_call(kernel, out_shape=jax.ShapeDtypeStruct((64, 2048), BF16),...  125 us

profile of v2, /device:TPU:1, one launch (start us, length us, event | category | flops | bytes accessed | tf_op | source)
XLA Modules:
  0.0 126.6 jit_solution(15860413898854546174)
XLA Ops:
  0.0 125.0 %layer.1 = bf16[64,2048]{1,0:T(8,128)(2,1)} custom-call(bf16[256,256]{1,0:T(8,128)(2,1)} %q_a.1, bf16[64,256]{1,0:T(8,128)(2,1)} %bitcast.9, bf16[64,256]{1,0:T(8,128)(2,1)} %bitcast.10, bf16[256,256]{1,0:T(8,128)(2,1)} %q_b.1, bf16[256,128]{1,0:T(8,128)(2,1)} %k_b.1, bf16[256,128]{1,0:T(8,128)(2,1)} %v_b.1, f32[64,8,128]{2,1,0:T(8,128)} %constant.8.clone.ra_h, ...), custom_call_target="tpu_custom_call" | custom-call | tf_op jit(solution)/shard_map/layer/pallas_call | solution.py:611
  125.0 1.7 %copy.25 = bf16[64,2048]{1,0:T(8,128)(2,1)} copy(bf16[64,2048]{1,0:T(8,128)(2,1)} %layer.1) | data formatting | bytes 524288

commit v3 on v2

--- a/solution.py
+++ b/solution.py
@@ -15,6 +15,8 @@
 NX = 4
 NY = 4
 NSETS = NZ
+W_START = 1
+W_FIRST = 3
 MESH = pl.DeviceIdType.MESH
 F32 = jnp.float32
 BF16 = jnp.bfloat16
@@ -118,10 +120,12 @@
         self.c_ax(0).start()
         self.c_ax(2).start()
 
-    def x_a(self):
-        p = self.p
+    def x_a1(self):
         self.c_ax(0).wait_recv()
         self.c_ax(1).start()
+
+    def x_a2(self):
+        p = self.p
         self.c_ax(2).wait_recv()
         self.c_ax(1).wait_recv()
         self.c_az(1, p.zz(p.s), p.z).start()
@@ -196,7 +200,7 @@
 
 def kernel(q_a, k_a, v_a, q_b, k_b, v_b, ra_h, rb_h, col_a, col_b, g_qa, g_ka, g_qb, g_kb, wg_h, wu_h, wd_h, woa_h, wob_h, x_ref, gain_ref, cg_ref, cu_ref, out_ref,
            qa_in, ka_in, va_in, qb_in, kb_in, vb_in, ra, rb, qa_ref, qb_ref, ba, bb, wa, wb, woa, wob, s_a, s_b, p_ref, acc_a, acc_b, mx,
-           attn, part, rs_mid, rs_in, mid, ag, pre, halo, hid, part2, rs_mid2, rs_in2,
+           attn, part, rs_mid, rs_in, mid, ag, pre, edge, hid, part2, rs_mid2, rs_in2,
            in_sem, loc, wo_sem, rs_s, rs_r, rs_s2, rs_r2, ag_s, ag_r, h_s, h_r, *sems):
     p = Place()
     n = len(sems) // 2
@@ -225,6 +229,9 @@
         pl.semaphore_signal(barrier, inc=1, device_id={"sp": sp}, device_id_type=MESH)
     for y in (up, down):
         pl.semaphore_signal(barrier, inc=1, device_id={"tp": y}, device_id_type=MESH)
+    for sp in (sp_next, sp_prev):
+        for y in (up, down, opp):
+            pl.semaphore_signal(barrier, inc=1, device_id={"sp": sp, "tp": y}, device_id_type=MESH)
 
     lane = lax.broadcasted_iota(jnp.int32, (64, 128), 1)
     first_head = lane < 64
@@ -275,7 +282,7 @@
     vt = vb_in[...].astype(F32).T.astype(BF16)
     slot_b[256:384, :] = vt[:, 0:128]
     slot_b[384:512, :] = vt[:, 128:256]
-    pl.semaphore_wait(barrier, 9)
+    pl.semaphore_wait(barrier, 15)
 
     g = Gather(p, lambda z, c: ba.at[c, z], lambda z, x, c: ba.at[c, z, x], lambda z, x, c: bb.at[c, z, x], sems[:n])
     w = Gather(p, lambda z, c: wa.at[pl.ds(z * NX, NX), c], lambda z, x, c: wa.at[z * NX + x, c],
@@ -302,7 +309,8 @@
     acc_a[...] = jnp.zeros_like(acc_a)
     acc_b[...] = jnp.zeros_like(acc_b)
     mx[...] = jnp.full_like(mx, -1e30)
-    g.x_a()
+    g.x_a1()
+    g.x_a2()
     for copy in (own_g, own_ua, own_ub, own_d):
         copy.wait()
     g.x1(0)
@@ -359,6 +367,13 @@
         else:
             acc_b[tile - 4] = acc_b[tile - 4] * factor + total
 
+    def both_sets(event, t):
+        event(t)
+
+        @pl.when(t + 1 < NSETS)
+        def _():
+            event(t + 1)
+
     @pl.loop(1, NSETS + 1)
     def _(t):
         odd = t % 2 == 1
@@ -370,6 +385,11 @@
         def _():
             g.x1(t)
             g.x2(t)
+
+            @pl.when(t + 1 < NSETS)
+            def _():
+                g.x1(t + 1)
+                g.x2(t + 1)
 
         bufs = (s_a, s_b)
         top = scores(0, bufs[0], parts)
@@ -386,20 +406,28 @@
                     def _():
                         g.z_a(t + 1)
 
-                @pl.when(t == 4)
+                @pl.when(t == W_START)
                 def _():
                     w.start_a()
                     w.start_b()
             if i == 3:
-                @pl.when(jnp.logical_and(odd, t + 1 < NSETS))
+                @pl.when(t == W_FIRST - 1)
                 def _():
-                    g.x1(t + 1)
-                    g.x2(t + 1)
-
-                @pl.when(t == 6)
+                    w.x_a1()
+                    w.x1(0)
+
+                @pl.when(t == W_FIRST)
                 def _():
-                    w.x_a()
-                    w.x1(0)
+                    w.x_a2()
+
+                @pl.when(jnp.logical_and(odd, t > W_FIRST))
+                def _():
+                    both_sets(w.z_b, t - W_FIRST - 1)
+                    both_sets(w.z_a, t - W_FIRST - 1)
+
+                @pl.when(jnp.logical_and(jnp.logical_not(odd), t > W_FIRST + 2))
+                def _():
+                    both_sets(w.x1, t - W_FIRST - 2)
             if i == 5:
                 @pl.when(jnp.logical_and(odd, t + 2 < NSETS))
                 def _():
@@ -408,22 +436,6 @@
                     @pl.when(t + 3 < NSETS)
                     def _():
                         g.z_b(t + 3)
-
-    def w_b(t):
-        for u in (t, t + 1):
-            if u < NSETS:
-                w.z_b(u)
-
-    def w_a(t):
-        for u in (t, t + 1):
-            if u < NSETS:
-                w.z_a(u)
-
-    def w_x(t):
-        for u in (t, t + 1):
-            if u < NSETS:
-                w.x1(u)
-
 
     o_a = [acc_a[h, 0:64, :] / acc_a[h, 64:65, :] for h in range(4)]
     attn[:, 0:256] = jnp.concatenate(o_a, axis=0).T.astype(BF16)
@@ -468,11 +480,20 @@
 
     first = reduce_copies(part, rs_mid, rs_in, rs_s, rs_r)
     reduce_first(first)
-    w_b(1)
-    w_a(1)
-    w_x(1)
+    left = [u for u in (1, 3, 5, 7) if u > 6 - W_FIRST + 0]
+
+    def weights_pair(t, events):
+        for event in events:
+            for u in (t, t + 1):
+                if u < NSETS:
+                    event(u)
+
+    for u in left[:-1]:
+        weights_pair(u, (w.z_b, w.z_a))
     reduce_second(first, part, rs_mid)
-    w_b(3)
+    for u in left[:-1]:
+        weights_pair(u, (w.x1,))
+    weights_pair(7, (w.z_b, w.z_a))
     reduce_last(first)
 
     def own_sum(src, ins, h):
@@ -499,19 +520,25 @@
         ag_copy(0, p.y, 0, up), ag_copy(1, p.y, 1, down), ag_copy(2, p.y, 1, up), ag_copy(3, p.y, 0, down),
         ag_copy(4, down, 0, up), ag_copy(5, up, 1, down),
     )
+    def edge_copy(k, y):
+        src, sp = (ag.at[3, :, pl.ds(48, 16)], sp_next) if k == 0 else (ag.at[0, :, pl.ds(0, 16)], sp_prev)
+        return pltpu.make_async_remote_copy(src_ref=src, dst_ref=edge.at[k], send_sem=h_s.at[y], recv_sem=h_r.at[k],
+                                            device_id={"sp": sp, "tp": y}, device_id_type=MESH)
+
+    for k, y in ((0, 3), (1, 0)):
+        @pl.when(p.y == y)
+        def _():
+            for to in range(4):
+                edge_copy(k, to).start()
+
     for copy in gathers[:4]:
         copy.start()
 
-    w_a(3)
-    w_x(3)
+    weights_pair(7, (w.x1,))
     gathers[0].wait_recv()
     gathers[4].start()
     gathers[1].wait_recv()
     gathers[5].start()
-    for t in (5, 7):
-        w_b(t)
-        w_a(t)
-        w_x(t)
 
     @pl.loop(0, NSETS)
     def _(t):
@@ -524,8 +551,15 @@
 
     for copy in gathers[2:]:
         copy.wait_recv()
-
-    rows = [ag[:, h].reshape(256, 1024) for h in range(2)]
+    edge_copy(0, 0).wait_recv()
+    edge_copy(1, 0).wait_recv()
+    for k, y in ((0, 3), (1, 0)):
+        @pl.when(p.y == y)
+        def _():
+            for to in range(4):
+                edge_copy(k, to).wait_send()
+
+    rows = [jnp.concatenate([edge[0, h], ag[:, h].reshape(256, 1024), edge[1, h]], axis=0) for h in range(2)]
     for m in range(2):
         for k in range(3):
             cols = slice(k * 256, k * 256 + 256)
@@ -545,15 +579,6 @@
                 tile = o if tile is None else tile + o
             pre[:, m * 768 + k * 256:m * 768 + k * 256 + 256] = tile.astype(BF16)
 
-    def halo_copy(k, src, sp):
-        return pltpu.make_async_remote_copy(src_ref=src, dst_ref=halo.at[k], send_sem=h_s.at[k], recv_sem=h_r.at[k],
-                                            device_id={"sp": sp}, device_id_type=MESH)
-
-    halos = (halo_copy(0, pre.at[240:256, :], sp_next), halo_copy(1, pre.at[0:16, :], sp_prev))
-    for copy in halos:
-        copy.start()
-    for copy in halos:
-        copy.wait_recv()
     keep_prev = jnp.where(p.sp == 0, 0.0, 1.0).astype(F32)
     keep_next = jnp.where(p.sp == 63, 0.0, 1.0).astype(F32)
     row = lax.broadcasted_iota(jnp.int32, (256, 256), 0)
@@ -562,11 +587,10 @@
         for m, taps in ((0, cg_ref), (1, cu_ref)):
             cols = slice(m * 768 + k * 256, m * 768 + k * 256 + 256)
             tcols = slice(k * 256, k * 256 + 256)
-            now = pre[:, cols].astype(F32)
-            before = halo[0, :, cols].astype(F32)[15:16, :] * keep_prev
-            after = halo[1, :, cols].astype(F32)[0:1, :] * keep_next
-            prev = jnp.where(row == 0, before, pltpu.roll(now, 1, 0))
-            nxt = jnp.where(row == 255, after, pltpu.roll(now, 255, 0))
+            whole = pre[:, cols].astype(F32)
+            now = whole[16:272]
+            prev = jnp.where(row == 0, whole[15:16] * keep_prev, pltpu.roll(whole, 1, 0)[16:272])
+            nxt = jnp.where(row == 255, whole[272:273] * keep_next, pltpu.roll(whole, 287, 0)[16:272])
             mixed.append(prev * taps[0:1, tcols] + now * taps[1:2, tcols] + nxt * taps[2:3, tcols])
         gate, upv = mixed
         hid[:, k * 256:k * 256 + 256] = (gate / (1.0 + jnp.exp(-gate)) * upv).astype(BF16)
@@ -585,7 +609,7 @@
     for h in range(2):
         cols = slice(h * 1024, h * 1024 + 1024)
         out_ref[:, cols] = (mid[:, cols] + own_sum(part2, rs_in2, h)).astype(BF16)
-    for copy in (*first, *second, *gathers, *halos):
+    for copy in (*first, *second, *gathers):
         copy.wait_send()
 
 
@@ -603,9 +627,9 @@
         v((2048, 256), F32), v((2048, 256), F32), v((2048, 256), BF16),
         v((4, 80, 256), F32), v((2, 144, 256), F32), v((6, 1, 256), F32),
         v((256, 512), BF16), v((4, 2, 64, 1024), BF16), v((4, 64, 1024), BF16), v((4, 64, 1024), BF16),
-        v((64, 2048), F32), v((4, 2, 64, 1024), BF16), v((256, 1536), BF16), v((2, 16, 1536), BF16),
+        v((64, 2048), F32), v((4, 2, 64, 1024), BF16), v((288, 1536), BF16), v((2, 2, 16, 1024), BF16),
         v((256, 768), BF16), v((4, 2, 64, 1024), BF16), v((4, 64, 1024), BF16), v((4, 64, 1024), BF16),
-        d((8,)), d((4,)), d((2,)), d((6,)), d((6,)), d((6,)), d((6,)), d((6,)), d((6,)), d((2,)), d((2,)),
+        d((8,)), d((4,)), d((2,)), d((6,)), d((6,)), d((6,)), d((6,)), d((6,)), d((6,)), d((4,)), d((2,)),
         *gather_sems(), *gather_sems(),
     ]
     return pl.pallas_call(

time: 128 us -> 119 us (0.930)
  Pallas kernels: 125 us -> 117 us
    pallas_call x1, Pallas kernels: 125 us -> 117 us  [fused(): pl.pallas_call(kernel, out_shape=jax.ShapeDtypeStruct((64, 2048), BF16),...]
where the time goes in v3:
time: 119 us
  Pallas kernels  117 us (98%)
  local copies, waits for them, and re-layouts  1.67 us (1%)
    pallas_call x1, Pallas kernels, fused(): pl.pallas_call(kernel, out_shape=jax.ShapeDtypeStruct((64, 2048), BF16),...  117 us

profile of v3, /device:TPU:1, one launch (start us, length us, event | category | flops | bytes accessed | tf_op | source)
XLA Modules:
  0.0 118.9 jit_solution(8613115385745971321)
XLA Ops:
  0.0 117.2 %layer.1 = bf16[64,2048]{1,0:T(8,128)(2,1)} custom-call(bf16[256,256]{1,0:T(8,128)(2,1)} %q_a.1, bf16[64,256]{1,0:T(8,128)(2,1)} %bitcast.9, bf16[64,256]{1,0:T(8,128)(2,1)} %bitcast.10, bf16[256,256]{1,0:T(8,128)(2,1)} %q_b.1, bf16[256,128]{1,0:T(8,128)(2,1)} %k_b.1, bf16[256,128]{1,0:T(8,128)(2,1)} %v_b.1, f32[64,8,128]{2,1,0:T(8,128)} %constant.8.clone.ra_h, ...), custom_call_target="tpu_custom_call" | custom-call | tf_op jit(solution)/shard_map/layer/pallas_call | solution.py:635
  117.2 1.7 %copy.25 = bf16[64,2048]{1,0:T(8,128)(2,1)} copy(bf16[64,2048]{1,0:T(8,128)(2,1)} %layer.1) | data formatting | bytes 524288

commit v4 on v3

--- a/solution.py
+++ b/solution.py
@@ -310,10 +310,10 @@
     acc_b[...] = jnp.zeros_like(acc_b)
     mx[...] = jnp.full_like(mx, -1e30)
     g.x_a1()
+    g.x1(0)
     g.x_a2()
     for copy in (own_g, own_ua, own_ub, own_d):
         copy.wait()
-    g.x1(0)
     g.x2(0)
     g.z_b(1)
     g.z_b(2)
@@ -381,22 +381,28 @@
         g.x3(t - 1)
         g.arrived(t - 1)
 
-        @pl.when(odd)
-        def _():
-            g.x1(t)
-            g.x2(t)
-
-            @pl.when(t + 1 < NSETS)
-            def _():
-                g.x1(t + 1)
-                g.x2(t + 1)
-
         bufs = (s_a, s_b)
         top = scores(0, bufs[0], parts)
         for i in range(6):
             following = scores(i + 1, bufs[(i + 1) % 2], parts) if i < 5 else None
             weigh(i, bufs[i % 2], top, parts)
             top = following
+            if i == 0:
+                @pl.when(odd)
+                def _():
+                    g.x1(t)
+                    g.x2(t)
+
+                    @pl.when(t + 1 < NSETS)
+                    def _():
+                        g.x1(t + 1)
+                        g.x2(t + 1)
+
+                @pl.when(t == W_START)
+                def _():
+                    w.start_a()
+                    w.start_b()
+
             if i == 1:
                 @pl.when(odd)
                 def _():
@@ -406,11 +412,7 @@
                     def _():
                         g.z_a(t + 1)
 
-                @pl.when(t == W_START)
-                def _():
-                    w.start_a()
-                    w.start_b()
-            if i == 3:
+            if i == 2:
                 @pl.when(t == W_FIRST - 1)
                 def _():
                     w.x_a1()
@@ -420,14 +422,17 @@
                 def _():
                     w.x_a2()
 
+            if i == 3:
                 @pl.when(jnp.logical_and(odd, t > W_FIRST))
                 def _():
                     both_sets(w.z_b, t - W_FIRST - 1)
                     both_sets(w.z_a, t - W_FIRST - 1)
 
+            if i == 4:
                 @pl.when(jnp.logical_and(jnp.logical_not(odd), t > W_FIRST + 2))
                 def _():
                     both_sets(w.x1, t - W_FIRST - 2)
+
             if i == 5:
                 @pl.when(jnp.logical_and(odd, t + 2 < NSETS))
                 def _():
@@ -493,7 +498,6 @@
     reduce_second(first, part, rs_mid)
     for u in left[:-1]:
         weights_pair(u, (w.x1,))
-    weights_pair(7, (w.z_b, w.z_a))
     reduce_last(first)
 
     def own_sum(src, ins, h):
@@ -534,11 +538,12 @@
     for copy in gathers[:4]:
         copy.start()
 
-    weights_pair(7, (w.x1,))
+    weights_pair(7, (w.z_b, w.z_a))
     gathers[0].wait_recv()
     gathers[4].start()
     gathers[1].wait_recv()
     gathers[5].start()
+    weights_pair(7, (w.x1,))
 
     @pl.loop(0, NSETS)
     def _(t):

time: 119 us -> 119 us (level); the launches traced: 119 us -> 117 us
  Pallas kernels: 117 us -> 115 us
    pallas_call x1, Pallas kernels: 117 us -> 115 us  [fused(): pl.pallas_call(kernel, out_shape=jax.ShapeDtypeStruct((64, 2048), BF16),...]
where the time goes in v4:
time: 119 us; the launch traced here: 117 us
  Pallas kernels  115 us (97%)
  local copies, waits for them, and re-layouts  1.67 us (1%)
    pallas_call x1, Pallas kernels, fused(): pl.pallas_call(kernel, out_shape=jax.ShapeDtypeStruct((64, 2048), BF16),...  115 us

profile of v4, /device:TPU:1, one launch (start us, length us, event | category | flops | bytes accessed | tf_op | source)
XLA Modules:
  0.0 117.0 jit_solution(2611261561010011601)
XLA Ops:
  0.0 115.3 %layer.1 = bf16[64,2048]{1,0:T(8,128)(2,1)} custom-call(bf16[256,256]{1,0:T(8,128)(2,1)} %q_a.1, bf16[64,256]{1,0:T(8,128)(2,1)} %bitcast.9, bf16[64,256]{1,0:T(8,128)(2,1)} %bitcast.10, bf16[256,256]{1,0:T(8,128)(2,1)} %q_b.1, bf16[256,128]{1,0:T(8,128)(2,1)} %k_b.1, bf16[256,128]{1,0:T(8,128)(2,1)} %v_b.1, f32[64,8,128]{2,1,0:T(8,128)} %constant.8.clone.ra_h, ...), custom_call_target="tpu_custom_call" | custom-call | tf_op jit(solution)/shard_map/layer/pallas_call | solution.py:640
  115.3 1.7 %copy.25 = bf16[64,2048]{1,0:T(8,128)(2,1)} copy(bf16[64,2048]{1,0:T(8,128)(2,1)} %layer.1) | data formatting | bytes 524288
